TPU v7x, 256 devices: a 4x2x16 block of a 4x16x16 slice. The times are simulated.
256 devices in a mesh: grp: 2 (over y), kv: 32 (over z, core), tp: 4 (over x).
Axes of the slice: x: 4, y: 2, z: 16, core: 2. Of those that a mesh axis runs over, the one named last changes fastest.
The devices are a block of a 4x16x16 slice.
Arguments:
- tokens: bfloat16 [1408, 6, 4096], P(('grp', 'kv')), parts along dimension 0, may hold values from -6 to 6
- norm_gain: bfloat16 [4096], replicated, may hold values from 0.099609375 to 1.8984375
- w_query: bfloat16 [4096, 2048], P('kv', 'tp'), may hold values from -0.09375 to 0.09375
- w_key: bfloat16 [4096, 2048], P('kv', 'tp'), may hold values from -0.09375 to 0.09375
- w_value: bfloat16 [4096, 2048], P('kv', 'tp'), may hold values from -0.09375 to 0.09375
- w_igate: bfloat16 [4096, 16], P(None, 'tp'), may hold values from -0.09375 to 0.09375
- w_fgate: bfloat16 [4096, 16], P(None, 'tp'), may hold values from -0.09375 to 0.09375
- igate_bias: float32 [16], P('tp'), may hold values from -2 to 2
- fgate_bias: float32 [16], P('tp'), may hold values from 0.5 to 6
- head_gain: bfloat16 [2048], P('tp'), may hold values from 0.099609375 to 1.8984375
- w_out: bfloat16 [2048, 4096], P('tp', 'kv'), may hold values from -0.125 to 0.125
- state_matrix: float32 [1408, 16, 128, 128], P(('grp', 'kv'), 'tp'), parts along dimension 0, may hold values from -1.5 to 1.5
- state_norm: float32 [1408, 16, 128], P(('grp', 'kv'), 'tp'), parts along dimension 0, may hold values from -4 to 4
- state_max: float32 [1408, 16], P(('grp', 'kv'), 'tp'), parts along dimension 0, may hold values from -4 to 4
- prior_keys: bfloat16 [1408, 6, 2048], P(('grp', 'kv'), None, 'tp'), parts along dimension 0, may hold values from -6 to 6
- prior_values: bfloat16 [1408, 6, 2048], P(('grp', 'kv'), None, 'tp'), parts along dimension 0, may hold values from -6 to 6
- prior_igate: float32 [1408, 6, 16], P(('grp', 'kv'), None, 'tp'), parts along dimension 0, may hold values from -4 to 4
- prior_fgate: float32 [1408, 6, 16], P(('grp', 'kv'), None, 'tp'), parts along dimension 0, may hold values from 0 to 5
- accepted: int32 [1408], P(('grp', 'kv')), parts along dimension 0, may hold values from 0 to 6
Outputs:
- mixed: float32 [1408, 6, 4096], P(('grp', 'kv'), None, 'tp'), parts along dimension 0
- new_matrix: float32 [1408, 16, 128, 128], P(('grp', 'kv'), 'tp'), parts along dimension 0
- new_norm: float32 [1408, 16, 128], P(('grp', 'kv'), 'tp'), parts along dimension 0
- new_max: float32 [1408, 16], P(('grp', 'kv'), 'tp'), parts along dimension 0
There are 2 independent parts, one for each index of `grp`. A program takes and returns all parts, laid end to end along the dimension named above; an argument that names none is the same for every part. Nothing has to cross between parts.
Inputs may be any that keep to these rules, and one draw needn't show every extreme that they name: `accepted`: how many of the 6 proposals of the last step were kept, from the first on.
All inputs are finite; a program needn't handle non-finite values.
Results may differ from a plain program's by a relative error of at most 0.019.
Values may be sent and summed in bfloat16 or wider, within the bound.
A program may use at most 128 MiB of HBM per device.

v0:
```python
import jax
import jax.numpy as jnp
from jax import lax
from jax.sharding import PartitionSpec as P

EPS = 1e-06


def in_one_piece(arrays, axis, dim, along):
    both = jnp.concatenate(arrays, axis=along)
    out, at, gathered = (lax.all_gather(both, axis, axis=dim, tiled=True), 0, [])
    for a in arrays:
        gathered.append(lax.slice_in_dim(out, at, at + a.shape[along], axis=along))
        at += a.shape[along]
    return tuple(gathered)


def heads_first(array, heads):
    seqs_n, props, width = array.shape
    return (
        array.astype(jnp.float32)
        .reshape(seqs_n, props, heads, width // heads)
        .transpose(0, 2, 1, 3)
    )


def fold_prior(matrix, normer, stabil, keys, values, in_pre, forget_pre, accepted):
    positions = jnp.arange(keys.shape[2], dtype=jnp.int32)
    active_mask = positions[None, None, :] < accepted[:, None, None]
    log_forget = jnp.where(active_mask, jax.nn.log_sigmoid(forget_pre), 0.0)
    in_gate = jnp.where(active_mask, in_pre, -1e30)
    cum_forget = jnp.cumsum(log_forget, axis=-1)
    total_forget = cum_forget[..., -1]
    weight_log = total_forget[..., None] - cum_forget + in_gate
    new_stabil = jnp.maximum(total_forget + stabil, jnp.max(weight_log, axis=-1))
    carry_scale = jnp.exp(total_forget + stabil - new_stabil)
    weighted_keys = keys * jnp.exp(weight_log - new_stabil[..., None])[..., None]
    new_matrix = carry_scale[..., None, None] * matrix + jnp.einsum(
        "bhtd,bhte->bhde", weighted_keys, values
    )
    new_normer = carry_scale[..., None] * normer + jnp.sum(weighted_keys, axis=2)
    return (new_matrix, new_normer, new_stabil)


def read_block(matrix, normer, stabil, query, keys, values, in_pre, forget_pre):
    props = query.shape[2]
    cum_forget = jnp.cumsum(jax.nn.log_sigmoid(forget_pre), axis=-1)
    causal = jnp.tril(jnp.ones((props, props), jnp.bool_))
    log_decay = jnp.where(
        causal, cum_forget[..., :, None] - cum_forget[..., None, :] + in_pre[..., None, :], -1e30
    )
    inter = cum_forget + stabil[..., None]
    row_max = jnp.maximum(inter, jnp.max(log_decay, axis=-1))
    inter_scale = jnp.exp(inter - row_max)
    scores = jnp.einsum("bhtd,bhud->bhtu", query, keys)
    scores = scores * jnp.exp(log_decay - row_max[..., None])
    numerator = inter_scale[..., None] * jnp.einsum("bhtd,bhde->bhte", query, matrix)
    numerator = numerator + jnp.einsum("bhtu,bhue->bhte", scores, values)
    denominator = inter_scale * jnp.einsum("bhtd,bhd->bht", query, normer)
    denominator = denominator + jnp.sum(scores, axis=-1)
    return numerator / jnp.maximum(jnp.abs(denominator), jnp.exp(-row_max))[..., None]


def head_norm(cell, head_gain):
    seqs_n, heads, props, width = cell.shape
    scaled = cell * lax.rsqrt(jnp.mean(cell * cell, axis=-1, keepdims=True) + EPS)
    scaled = scaled.transpose(0, 2, 1, 3).reshape(seqs_n * props, heads * width)
    return (scaled * head_gain.astype(jnp.float32)).astype(jnp.bfloat16)


def body(
    tokens,
    norm_gain,
    w_query,
    w_key,
    w_value,
    w_igate,
    w_fgate,
    igate_bias,
    fgate_bias,
    head_gain,
    w_out,
    state_matrix,
    state_norm,
    state_max,
    prior_keys,
    prior_values,
    prior_igate,
    prior_fgate,
    accepted,
):
    seq_count, props, width = tokens.shape
    local_heads = state_matrix.shape[1]
    key_size = state_matrix.shape[2]
    row_count = seq_count * props
    inputs = tokens.astype(jnp.float32)
    normed = inputs * lax.rsqrt(jnp.mean(inputs * inputs, axis=-1, keepdims=True) + EPS)
    normed_rows = (
        (normed * norm_gain.astype(jnp.float32)).astype(jnp.bfloat16).reshape(row_count, width)
    )
    pieces = in_one_piece((w_query, w_key, w_value), "kv", 0, 1)
    query_sum, key_sum, value_sum = tuple(
        (jnp.dot(normed_rows, piece, preferred_element_type=jnp.float32) for piece in pieces)
    )
    query = query_sum.astype(jnp.bfloat16).reshape(seq_count, props, -1)
    keys = key_sum.astype(jnp.bfloat16).reshape(seq_count, props, -1)
    values = value_sum.astype(jnp.bfloat16).reshape(seq_count, props, -1)
    in_pre = jnp.dot(normed_rows, w_igate, preferred_element_type=jnp.float32) + igate_bias
    forget_pre = jnp.dot(normed_rows, w_fgate, preferred_element_type=jnp.float32) + fgate_bias
    in_pre = in_pre.reshape(seq_count, props, local_heads).transpose(0, 2, 1)
    forget_pre = forget_pre.reshape(seq_count, props, local_heads).transpose(0, 2, 1)
    new_matrix, new_normer, new_stabil = fold_prior(
        state_matrix,
        state_norm,
        state_max,
        heads_first(prior_keys, local_heads) * key_size ** (-0.5),
        heads_first(prior_values, local_heads),
        prior_igate.transpose(0, 2, 1),
        prior_fgate.transpose(0, 2, 1),
        accepted,
    )
    cell = read_block(
        new_matrix,
        new_normer,
        new_stabil,
        heads_first(query, local_heads),
        heads_first(keys, local_heads) * key_size ** (-0.5),
        heads_first(values, local_heads),
        in_pre,
        forget_pre,
    )
    hidden = head_norm(cell, head_gain)
    partial_out = jnp.dot(
        hidden, lax.all_gather(w_out, "kv", axis=1, tiled=True), preferred_element_type=jnp.float32
    )
    mixed = lax.psum_scatter(partial_out, "tp", scatter_dimension=1, tiled=True)
    return (mixed.reshape(seq_count, props, -1), new_matrix, new_normer, new_stabil)


def solution(mesh):
    return jax.shard_map(
        body,
        mesh=mesh,
        in_specs=(
            P(("grp", "kv"), None, None),
            P(),
            P("kv", "tp"),
            P("kv", "tp"),
            P("kv", "tp"),
            P(None, "tp"),
            P(None, "tp"),
            P("tp"),
            P("tp"),
            P("tp"),
            P("tp", "kv"),
            P(("grp", "kv"), "tp", None, None),
            P(("grp", "kv"), "tp", None),
            P(("grp", "kv"), "tp"),
            P(("grp", "kv"), None, "tp"),
            P(("grp", "kv"), None, "tp"),
            P(("grp", "kv"), None, "tp"),
            P(("grp", "kv"), None, "tp"),
            P(("grp", "kv")),
        ),
        out_specs=(
            P(("grp", "kv"), None, "tp"),
            P(("grp", "kv"), "tp", None, None),
            P(("grp", "kv"), "tp", None),
            P(("grp", "kv"), "tp"),
        ),
        check_vma=False,
    )
```

profile of v0, /device:TPU:43, one launch (start us, length us, event | category | flops | bytes accessed | tf_op | source)
XLA Modules:
  0.0 230.6 jit_solution(13172241641892140471)
XLA Ops:
  7.2 0.0 copy-start
  7.2 0.1 all-gather.3.cloned.1.call-start
  7.3 1.9 pad_maximum_fusion
  9.2 0.1 all-gather.3.cloned.1.call-update
  9.2 0.1 all-gather.5.cloned.1.call-start
  9.3 0.7 all-gather.5.cloned.1.call-update
  10.0 0.1 reduce-scatter.2.cloned.1.call-start
  10.1 0.7 convert_element_type.40
  10.8 0.7 iota_compare_fusion.1
  11.4 0.7 fusion.52
  12.2 0.1 copy.128
  12.3 0.7 fusion.79
  13.0 0.1 copy.157
  13.1 0.8 copy.129
  13.9 0.1 copy.131
  14.0 0.7 convert_element_type.34
  14.7 1.0 reshape.110
  15.7 1.0 reshape.114
  16.7 0.3 fusion.6
  17.0 0.4 fusion.8
  17.4 0.0 copy-start.7
  17.4 0.6 copy.126
  18.0 0.0 copy-start.5
  18.0 0.0 copy-start.8
  18.1 0.0 copy-start.2
  18.1 0.4 reshape.106
  18.5 0.0 copy-start.3
  18.5 0.4 fusion.24
  18.9 0.1 neg.38
  19.0 0.1 copy.127
  19.1 0.1 copy.132
  19.3 0.4 convolution_add_fusion
  19.7 0.1 reshape.107
  19.8 0.3 fusion.30
  20.1 0.1 copy.135
  20.2 0.1 copy.139
  20.4 0.1 copy.143
  20.5 0.2 fusion.29
  20.7 0.1 multiply_add_fusion.1
  20.8 0.0 copy-start.4
  20.8 7.5 %multiply_add_fusion = f32[22,4,128,128]{3,2,1,0:T(8,128)} fusion(f32[22,4,128,128]{3,2,1,0:T(8,128)} %param.30, f32[22,4]{1,0:T(8,128)S(1)} %get-tuple-element.30, f32[22,6,4,128]{3,2,0,1:T(4,128)S(1)} %reshape.114, bf16[22,6,4,128]{3,2,0,1:T(4,128)(2,1)S(1)} %reshape.110, f32[22,4,6]{2,1,0:T(4,128)S(1)} %copy.139), kind=kOutput, calls=%fused_computation | convolution fusion | flops 20252672 | bytes 11942304 | tf_op jit(solution)/shard_map/bhtd,bhte->bhde/dot_general | solution.py:38
  28.3 80.9 %all-gather.3.cloned.1.call-done = bf16[4096,1536]{1,0:T(8,128)(2,1)} async-done(((bf16[128,1536]{1,0:T(8,128)(2,1)}), bf16[4096,1536]{1,0:T(8,128)(2,1)}) %all-gather.3.cloned.1.call-update) | async-done | bytes 12582928 | tf_op jit(solution)/shard_map/all_gather | solution.py:11
  109.2 3.0 %fusion.21 = bf16[132,512]{1,0:T(8,128)(2,1)S(1)} fusion(bf16[132,4096]{1,0:T(8,128)(2,1)S(1)} %reshape.106, bf16[4096,1536]{1,0:T(8,128)(2,1)} %all-gather.3.cloned.1.call-done), kind=kOutput, calls=%fused_computation.17 | convolution fusion | flops 553715712 | bytes 5410816 | tf_op jit(solution)/shard_map/dot_general | solution.py:103
  112.2 3.0 %fusion.9 = bf16[132,512]{1,0:T(8,128)(2,1)S(1)} fusion(bf16[132,4096]{1,0:T(8,128)(2,1)S(1)} %reshape.106, bf16[4096,1536]{1,0:T(8,128)(2,1)} %all-gather.3.cloned.1.call-done), kind=kOutput, calls=%fused_computation.13 | convolution fusion | flops 553715712 | bytes 5410816 | tf_op jit(solution)/shard_map/dot_general | solution.py:103
  115.2 3.0 %fusion.18 = bf16[132,512]{1,0:T(8,128)(2,1)S(1)} fusion(bf16[132,4096]{1,0:T(8,128)(2,1)S(1)} %reshape.106, bf16[4096,1536]{1,0:T(8,128)(2,1)} %all-gather.3.cloned.1.call-done), kind=kOutput, calls=%fused_computation.16 | convolution fusion | flops 553918464 | bytes 5410816 | tf_op jit(solution)/shard_map/dot_general | solution.py:103
  118.2 0.4 fusion.82
  118.6 0.1 copy.146
  118.7 0.2 fusion.34
  119.0 0.1 copy.156
  119.1 0.1 copy.136
  119.3 0.1 copy.150
  119.4 0.1 copy.147
  119.5 0.1 copy.148
  119.6 3.5 %fusion.37 = f32[22,4,6,128]{3,2,1,0:T(8,128)S(1)} fusion(f32[22,4,128,128]{3,2,1,0:T(8,128)} %multiply_add_fusion, bf16[22,6,4,128]{3,2,1,0:T(4,128)(2,1)S(1)} %reshape.108), kind=kOutput, calls=%fused_computation.40 | convolution fusion | flops 17301504 | bytes 6172672 | tf_op jit(solution)/shard_map/bhtd,bhde->bhte/dot_general | solution.py:57
  123.1 0.5 multiply_reduce_fusion
  123.7 0.3 fusion.26
  124.0 0.1 copy.151
  124.1 0.1 pad.3
  124.2 62.2 %all-gather.5.cloned.1.call-done = bf16[512,4096]{1,0:T(8,128)(2,1)} async-done(((bf16[512,128]{1,0:T(8,128)(2,1)}), bf16[512,4096]{1,0:T(8,128)(2,1)}) %all-gather.5.cloned.1.call-update) | async-done | bytes 4194320 | tf_op jit(solution)/shard_map/all_gather | solution.py:134
  186.4 4.3 %fusion.45 = f32[132,4096]{1,0:T(8,128)} fusion(bf16[512,4096]{1,0:T(8,128)(2,1)} %all-gather.5.cloned.1.call-done, f32[132,512]{1,0:T(8,128)S(1)} %bitcast.154, f32[512]{0:T(512)S(1)} %convert_element_type.40), kind=kOutput, calls=%fused_computation.48 | convolution fusion | flops 553783296 | bytes 6629376 | tf_op jit(solution)/shard_map/dot_general | solution.py:133
  190.8 0.1 reduce-scatter.2.cloned.1.call-update
  190.8 31.0 %reduce-scatter.2.cloned.1.call-done = f32[132,1024]{1,0:T(8,128)} async-done(((f32[132,4096]{1,0:T(8,128)}), f32[132,1024]{1,0:T(8,128)}) %reduce-scatter.2.cloned.1.call-update) | async-done | bytes 540688 | tf_op jit(solution)/shard_map/reduce_scatter | solution.py:136
  221.8 1.1 reshape.113
  223.0 1.1 copy.152
  (25 shorter events, 0.3 us)
Async XLA Ops:
  7.2 11.3 %copy-start = (bf16[4096,4]{0,1:T(4,128)(2,1)S(1)}, bf16[4096,4]{0,1:T(4,128)(2,1)}, u32[]{:S(2)}) copy-start(bf16[4096,4]{0,1:T(4,128)(2,1)} %param.25) | copy-start | bytes 98308
  7.2 9.5 %copy-start.1 = (bf16[22,6,4096]{2,0,1:T(8,128)(2,1)S(1)}, bf16[22,6,4096]{2,0,1:T(8,128)(2,1)}, u32[]{:S(2)}) copy-start(bf16[22,6,4096]{2,0,1:T(8,128)(2,1)} %param.19) | copy-start | bytes 3244036
  7.2 102.0 %all-gather.3.cloned.1.call-start = ((), (), s32[]{:S(2)}) async-start(), calls=%async_computation.1 | async-start | bytes 12976128 | tf_op jit(solution)/shard_map/all_gather | solution.py:11
  9.2 177.2 %all-gather.5.cloned.1.call-start = ((), (), s32[]{:S(2)}) async-start(), calls=%async_computation.2 | async-start | bytes 4325376 | tf_op jit(solution)/shard_map/all_gather | solution.py:134
  10.0 211.8 %reduce-scatter.2.cloned.1.call-start = ((), (), s32[]{:S(2)}) async-start(), calls=%async_computation.3 | async-start | bytes 2785280 | tf_op jit(solution)/shard_map/reduce_scatter | solution.py:136
  14.0 105.2 %copy-start.6 = (f32[22,4]{0,1:T(4,128)}, f32[22,4]{0,1:T(4,128)S(1)}, u32[]{:S(2)}) copy-start(f32[22,4]{0,1:T(4,128)S(1)} %copy.131) | copy-start | bytes 1060
  17.4 1.0 copy-start.7
  18.0 1.2 copy-start.5
  18.0 1.2 copy-start.8
  18.1 2.2 copy-start.2
  18.5 2.2 copy-start.3
  20.8 97.9 %copy-start.4 = (f32[22,4,128]{2,1,0:T(4,128)}, f32[22,4,128]{2,1,0:T(4,128)S(1)}, u32[]{:S(2)}) copy-start(f32[22,4,128]{2,1,0:T(4,128)S(1)} %multiply_add_fusion.1) | copy-start | bytes 135172
Sparse Core Ops, SparseCore 0:
  10.5 98.6 all-gather.2
  111.0 75.4 all-gather.4
  191.0 30.8 reduce-scatter.1
where the time goes:
time: 234 us; the launch traced here: 231 us
  waiting for transfers between devices  175 us (75%)
  matrix products  26.2 us (11%)
  between operations  14.1 us (6%)
  local copies, waits for them, and re-layouts  8.09 us (3%)
  other arithmetic  7.18 us (3%)
    all_gather x1, waiting for transfers between devices, in_one_piece(): lax.all_gather(both, axis, axis=dim, tiled=True)  80.9 us
    all_gather x1, waiting for transfers between devices, body(): lax.all_gather(w_out, 'kv', axis=1, tiled=True)  62.2 us
    reduce_scatter x1, waiting for transfers between devices, body(): mixed = lax.psum_scatter(partial_out, 'tp', scatter_dimension=1, tiled=True)  31 us
    dot_general x3, matrix products, body(): jnp.dot(normed_rows, piece, preferred_element_type=jnp.float32)  8.9 us
    dot_general x1, matrix products, fold_prior(): jnp.einsum('bhtd,bhte->bhde', weighted_keys, values)  7.52 us
  transfers between devices with their start and end apart: 3, of which 3 were waited for; matrix products, arithmetic and copies ran while one was open for 14% of the time, Pallas kernels for 0%

commit v1 on v0

v1 whole, which is shorter than its diff:
```python
import functools

import jax
import jax.numpy as jnp
from jax import lax
from jax.experimental import pallas as pl
from jax.experimental.pallas import tpu as pltpu
from jax.sharding import PartitionSpec as P

EPS = 1e-06
F32, BF16 = jnp.float32, jnp.bfloat16
MESH = pl.DeviceIdType.MESH
CORES = 2
HIGH = lax.Precision.HIGHEST
LAST = (((1,), (1,)), ((), ()))


def log_sigmoid(v):
    return jnp.minimum(v, 0.0) - jnp.log1p(jnp.exp(-jnp.abs(v)))


def kernel(
    dims,
    tok_h, ngain, wq_h, wk_h, wv_h, wig_h, wfg_h, igb, fgb, hgain, wo_h, st_h, sn_h, smax,
    pk_h, pv_h, pig, pfg, acc_n,
    mixed, nmat_h, nnorm, nmax,
    tok, xf, xb, wg, wo, acc, st, sb, pk, pv, sn, wig, wfg, kwb, vb, qb, qsb, gr, gc, ab, nrm,
    qall, sendq, hid, rsend, rrecv, own,
    loc, zs, zr, dsn, drc, xs, xr, qs_sem, qr_sem, rs_sem, rr_sem, ms,
):
    B, T, BP, NZ, TPN, HL, DK = dims
    R = T * BP
    g, kv, tp = lax.axis_index("grp"), lax.axis_index("kv"), lax.axis_index("tp")
    z, c = kv // CORES, lax.rem(kv, CORES)
    par = lax.rem(g, 2)
    mate = g + 1 - 2 * par
    KC = wq_h.shape[0]
    ZC = CORES * KC
    CW = wq_h.shape[1] // 2
    OC = wo_h.shape[1]
    HO = wo_h.shape[0] // 2
    LASTS = NZ // 2

    def zat(s, way):
        return lax.rem(z + NZ - s, NZ) if way == 0 else lax.rem(z + s, NZ)

    ring_to = (lax.rem(z + 1, NZ) * CORES + c, lax.rem(z + NZ - 1, NZ) * CORES + c)
    twin = z * CORES + 1 - c

    def slot(item, zz, cc):
        if item < 3:
            return wg.at[
                pl.ds(pl.multiple_of(zz * ZC + cc * KC, KC), KC), pl.ds(item * CW, CW)
            ]
        return wo.at[zz, pl.ds((item - 3) * HO, HO), pl.ds(pl.multiple_of(cc * OC, OC), OC)]

    def zcopy(item, way, s, shard):
        ref = slot(item, zat(shard, way), c)
        return pltpu.make_async_remote_copy(
            src_ref=ref, dst_ref=ref, send_sem=zs.at[item, way, s], recv_sem=zr.at[item, way, s],
            device_id={"kv": ring_to[way]}, device_id_type=MESH,
        )

    def dcopy(item, way, s, cc):
        ref = slot(item, zat(s, way), cc)
        return pltpu.make_async_remote_copy(
            src_ref=ref, dst_ref=ref, send_sem=dsn.at[item, way, s], recv_sem=drc.at[item, way, s],
            device_id={"kv": twin}, device_id_type=MESH,
        )

    def xcopy(zz, lo, hi):
        return pltpu.make_async_remote_copy(
            src_ref=xb.at[zz, pl.ds(lo, R), :], dst_ref=xb.at[zz, pl.ds(hi, R), :],
            send_sem=xs.at[zz], recv_sem=xr.at[zz],
            device_id={"grp": mate}, device_id_type=MESH,
        )

    def step(items, s, last_plus, last_minus, has_minus):
        for item in items:
            zcopy(item, 0, s - 1, s).wait_recv()
            if not last_plus:
                zcopy(item, 0, s, s).start()
            dcopy(item, 0, s, c).start()
            if has_minus:
                zcopy(item, 1, s - 1, s).wait_recv()
                if not last_minus:
                    zcopy(item, 1, s, s).start()
                dcopy(item, 1, s, c).start()

    def begin(items):
        for item in items:
            for way in (0, 1):
                zcopy(item, way, 0, 0).start()
            dcopy(item, 0, 0, c).start()

    def product(s, way):
        zz = zat(s, way)
        for item in range(3):
            dcopy(item, way, s, 1 - c).wait_recv()
        xcopy(zz, R, R).wait_recv()
        rows = pl.ds(pl.multiple_of(zz * ZC, ZC), ZC)
        return jnp.dot(xb[zz], wg[rows, :], preferred_element_type=F32)

    c0 = pl.multiple_of(par * CW, CW)
    mine = [
        pltpu.make_async_copy(src.at[:, pl.ds(c0, CW)], slot(i, z, c), loc.at[i])
        for i, src in enumerate((wq_h, wk_h, wv_h))
    ] + [
        pltpu.make_async_copy(wo_h.at[pl.ds(i * HO, HO), :], slot(3 + i, z, c), loc.at[3 + i])
        for i in range(2)
    ]
    loads = [
        pltpu.make_async_copy(src, dst, loc.at[5 + i])
        for i, (src, dst) in enumerate((
            (tok_h, tok), (wig_h, wig), (wfg_h, wfg), (pk_h, pk), (pv_h, pv), (sn_h, sn), (st_h, st),
        ))
    ]
    for cp in mine + loads:
        cp.start()
    barrier = pltpu.get_barrier_semaphore()
    for dev in (
        [{"kv": ring_to[0]}, {"kv": ring_to[1]}, {"kv": twin}, {"grp": mate}]
        + [{"tp": lax.rem(tp + d, TPN)} for d in range(1, TPN)]
    ):
        pl.semaphore_signal(barrier, inc=1, device_id=dev, device_id_type=MESH)
    for cp in mine:
        cp.wait()
    pl.semaphore_wait(barrier, 3 + TPN)
    begin((0, 1, 2))

    loads[0].wait()
    xf[...] = jnp.zeros_like(xf)

    def norm_rows(t, carry):
        v = tok[t].astype(F32)
        v = v * lax.rsqrt(jnp.mean(v * v, axis=-1, keepdims=True) + EPS) * ngain[...].astype(F32)
        xf[t, :B, :] = v
        return carry

    lax.fori_loop(0, T, norm_rows, 0)

    def cut_rows(i, carry):
        cols = pl.ds(pl.multiple_of(i * ZC, ZC), ZC)
        xb[i, :R, :] = xf[:, :, cols].reshape(R, ZC).astype(BF16)
        return carry

    lax.fori_loop(0, NZ, cut_rows, 0)
    for s in range(LASTS + 1):
        for way in (0, 1):
            if way == 0 or 0 < s < LASTS:
                xcopy(zat(s, way), 0, R).start()

    loads[1].wait()
    loads[2].wait()

    def gates(i, carry):
        a0, a1, b0, b1 = carry
        cols = pl.ds(pl.multiple_of(i * ZC, ZC), ZC)
        xi, wi, wf = xb[i, :R, :], wig[:, cols], wfg[:, cols]
        dot = functools.partial(lax.dot_general, dimension_numbers=LAST, preferred_element_type=F32)
        return a0 + dot(xi, wi), a1 + dot(xi, wf), b0 + dot(wi, xi), b1 + dot(wf, xi)

    zr_, zc_ = jnp.zeros((R, HL), F32), jnp.zeros((HL, R), F32)
    _, fr, ic, fc = lax.fori_loop(0, NZ, gates, (zr_, zr_, zc_, zc_))
    r0 = lax.broadcasted_iota(jnp.int32, (R, R), 0)
    r1 = lax.broadcasted_iota(jnp.int32, (R, R), 1)
    same = lax.rem(r0, BP) == lax.rem(r1, BP)
    upto = jnp.where(same & (r0 >= r1), 1.0, 0.0).astype(F32)
    cum_r = jnp.dot(
        upto, log_sigmoid(fr + fgb[...]), precision=HIGH, preferred_element_type=F32
    )
    lane_of = lambda ref: jnp.concatenate(
        [jnp.broadcast_to(ref[:, h : h + 1], (1, R)) for h in range(HL)], axis=0
    )
    cum_c = lax.dot_general(
        log_sigmoid(fc + lane_of(fgb)), upto, LAST, precision=HIGH, preferred_element_type=F32
    )
    gc[:HL, :] = ic + lane_of(igb) - cum_c

    lf, ig, run = [], [], None
    for t in range(T):
        live = t < acc_n[...]
        f = jnp.where(live, log_sigmoid(pfg[t]), 0.0)
        run = f if run is None else run + f
        lf.append(run)
        ig.append(jnp.where(live, pig[t], -1e30))
    wlog = [run - lf[t] + ig[t] for t in range(T)]
    top = functools.reduce(jnp.maximum, wlog)
    new_max = jnp.maximum(run + smax[...], top)
    nmax[...] = new_max
    eye = jnp.where(
        lax.broadcasted_iota(jnp.int32, (BP, B), 0) == lax.broadcasted_iota(jnp.int32, (BP, B), 1),
        1.0, 0.0,
    ).astype(F32)
    turn = lambda v: lax.dot_general(eye, v, LAST, precision=HIGH, preferred_element_type=F32)
    carry_r = turn(jnp.exp(run + smax[...] - new_max))
    max_r = turn(new_max)
    wts = [turn(jnp.exp(wlog[t] - new_max)) * (DK**-0.5) for t in range(T)]
    for h in range(HL):
        ab[h] = jnp.broadcast_to(carry_r[:, h : h + 1], (BP, DK))
        gr[h, 0] = jnp.broadcast_to(cum_r[:, h : h + 1], (R, DK))
        for t in range(T):
            gr[h, 1, t * BP : (t + 1) * BP] = jnp.broadcast_to(max_r[:, h : h + 1], (BP, DK))

    for cp in loads[3:6]:
        cp.wait()
    for ref in (kwb, vb, qb):
        ref[...] = jnp.zeros_like(ref)
    for h in range(HL):
        cols = slice(h * DK, (h + 1) * DK)
        total = None
        for t in range(T):
            kw = pk[t, :, cols].astype(F32) * wts[t][:B, h : h + 1]
            kwb[h, pl.ds(t, B, stride=8), :] = kw
            vb[h, pl.ds(t, B, stride=8), :] = pv[t, :, cols].astype(F32)
            total = kw if total is None else total + kw
        nrm[h, :B] = total
    for b in range(B):
        for h in range(HL):
            row = ab[h, b : b + 1] * sn[b, h : h + 1] + nrm[h, b : b + 1]
            nrm[h, b : b + 1] = row
            nnorm[b, h : h + 1] = row
    loads[6].wait()

    def fold(b):
        rows = pl.ds(pl.multiple_of(b * 8, 8), 8)
        for h in range(HL):
            outer = lax.dot_general(
                kwb[h, rows, :].astype(BF16), vb[h, rows, :].astype(BF16),
                (((0,), (0,)), ((), ())), preferred_element_type=F32,
            )
            s = st[b, h] * ab[h, pl.ds(b, 1), :] + outer
            st[b, h] = s
            sb[b, h] = s.astype(BF16)
        pltpu.make_async_copy(st.at[b], nmat_h.at[b], ms.at[b]).start()

    laps = LASTS - 3
    per = B // laps

    qkv = (0, 1, 2)
    step(qkv, 1, False, False, True)
    acc[...] = product(0, 0)
    for b in range(per * laps, B):
        fold(b)

    def ring(s, carry):
        step(qkv, s, False, False, True)
        acc[...] += product(s - 1, 0)
        acc[...] += product(s - 1, 1)
        for i in range(per):
            fold((s - 2) * per + i)
        return carry

    lax.fori_loop(2, LASTS - 1, ring, 0)
    step(qkv, LASTS - 1, False, True, True)
    begin((3, 4))
    acc[...] += product(LASTS - 2, 0)
    acc[...] += product(LASTS - 2, 1)
    step(qkv, LASTS, True, True, False)
    acc[...] += product(LASTS - 1, 0)
    acc[...] += product(LASTS - 1, 1)
    full = acc[...] + product(LASTS, 0)
    qcopies = []
    for j in range(3):
        cols = slice(j * CW, (j + 1) * CW)
        sendq[j] = full[R:, cols].astype(BF16)
        cp = pltpu.make_async_remote_copy(
            src_ref=sendq.at[j], dst_ref=qall.at[j, par], send_sem=qs_sem.at[j],
            recv_sem=qr_sem.at[j], device_id={"grp": mate}, device_id_type=MESH,
        )
        cp.start()
        qcopies.append(cp)
        qall[j, par] = full[:R, cols].astype(BF16)

    out_items = (3, 4)

    def out_step(s):
        step(out_items, s, s == LASTS, s >= LASTS - 1, s < LASTS)

    keep = same & (r0 >= r1) & (lax.rem(r1, BP) < B)

    def spread(half, i):
        h = half * 2 + i
        q = qall[0, half, :, i * DK : (i + 1) * DK].astype(F32)
        for t in range(T):
            qb[h, pl.ds(t, BP, stride=8), :] = q[t * BP : (t + 1) * BP]
        for b in range(B):
            rows = slice(b * 8, b * 8 + 8)
            qsb[h, rows, :] = jnp.dot(
                qb[h, rows, :].astype(BF16), sb[b, h], preferred_element_type=F32
            )

    def head(half, i):
        h = half * 2 + i
        cols = slice(i * DK, (i + 1) * DK)
        q, k, v = (qall[j, half, :, cols] for j in range(3))
        cum = gr[h, 0, :, :1]
        inter = cum + gr[h, 1, :, :1]
        decay = jnp.where(keep, cum + gc[pl.ds(h, 1), :], -1e30)
        top_r = jnp.maximum(inter, jnp.max(decay, axis=1, keepdims=True))
        scale = jnp.exp(inter - top_r)
        scores = lax.dot_general(q, k, LAST, preferred_element_type=F32) * (DK**-0.5)
        scores = scores * jnp.exp(decay - top_r)
        q32 = q.astype(F32)
        nh = nrm[h]
        read = jnp.concatenate(
            [qsb[h, pl.ds(t, BP, stride=8), :] for t in range(T)], axis=0
        )
        qn = jnp.concatenate(
            [
                jnp.sum(q32[t * BP : (t + 1) * BP] * nh, axis=1, keepdims=True)
                for t in range(T)
            ],
            axis=0,
        )
        num = scale * read + jnp.dot(scores.astype(BF16), v, preferred_element_type=F32)
        den = scale * qn + jnp.sum(scores, axis=1, keepdims=True)
        cell = num / jnp.maximum(jnp.abs(den), jnp.exp(-top_r))
        cell = cell * lax.rsqrt(jnp.mean(cell * cell, axis=1, keepdims=True) + EPS)
        hc = pl.ds(pl.multiple_of(h * DK, DK), DK)
        hid[:, hc] = (cell * hgain[:, hc].astype(F32)).astype(BF16)

    nrm[:, B:] = jnp.zeros((HL, BP - B, DK), F32)
    qsb[:, B * 8 :, :] = jnp.zeros((HL, (BP - B) * 8, DK), F32)
    spread(par, 0)
    out_step(1)
    spread(par, 1)
    out_step(2)
    head(par, 0)
    out_step(3)
    head(par, 1)
    for cp in qcopies:
        cp.wait_send()
    for j in range(3):
        pltpu.make_async_remote_copy(
            src_ref=sendq.at[j], dst_ref=qall.at[j, 1 - par], send_sem=qs_sem.at[j],
            recv_sem=qr_sem.at[j], device_id={"grp": mate}, device_id_type=MESH,
        ).wait_recv()
    out_step(4)
    spread(1 - par, 0)
    out_step(5)
    spread(1 - par, 1)
    out_step(6)
    head(1 - par, 0)
    out_step(7)
    head(1 - par, 1)
    out_step(8)
    for item in out_items:
        for s in range(LASTS + 1):
            dcopy(item, 0, s, 1 - c).wait_recv()
            if 0 < s < LASTS:
                dcopy(item, 1, s, 1 - c).wait_recv()

    per_tp = NZ // TPN
    NB = CORES * OC

    def block(target, i):
        return jnp.dot(hid[...], wo[target * per_tp + i], preferred_element_type=F32)

    sends = []
    for d in [TPN // 2] + [e for e in range(1, TPN) if e != TPN // 2]:
        target = lax.rem(tp + d, TPN)
        for i in range(per_tp):
            rsend[d - 1, :, i * NB : (i + 1) * NB] = block(target, i).astype(BF16)
        cp = pltpu.make_async_remote_copy(
            src_ref=rsend.at[d - 1], dst_ref=rrecv.at[d - 1], send_sem=rs_sem.at[d - 1],
            recv_sem=rr_sem.at[d - 1], device_id={"tp": target}, device_id_type=MESH,
        )
        cp.start()
        sends.append(cp)
    for i in range(per_tp):
        own[:, i * NB : (i + 1) * NB] = block(tp, i)

    def sent(s, carry):
        for item in range(5):
            for way in (0, 1):
                zcopy(item, way, s, s).wait_send()
                dcopy(item, way, s, c).wait_send()
        return carry

    for item in range(5):
        for way in (0, 1):
            zcopy(item, way, 0, 0).wait_send()
        dcopy(item, 0, 0, c).wait_send()
        zcopy(item, 0, LASTS - 1, LASTS - 1).wait_send()
        for way in (0, 1):
            dcopy(item, way, LASTS - 1, c).wait_send()
        dcopy(item, 0, LASTS, c).wait_send()
    lax.fori_loop(1, LASTS - 1, sent, 0)

    def x_sent(i, carry):
        xcopy(i, 0, R).wait_send()
        return carry

    lax.fori_loop(0, NZ, x_sent, 0)

    def m_sent(b, carry):
        pltpu.make_async_copy(st.at[b], nmat_h.at[b], ms.at[b]).wait()
        return carry

    lax.fori_loop(0, B, m_sent, 0)
    for cp in sends:
        cp.wait()
    for t in range(T):
        rows = slice(t * BP, (t + 1) * BP)
        total = own[rows]
        for d in range(TPN - 1):
            total = total + rrecv[d, rows].astype(F32)
        mixed[t] = total[:B]


def body(
    tokens, norm_gain, w_query, w_key, w_value, w_igate, w_fgate, igate_bias, fgate_bias,
    head_gain, w_out, state_matrix, state_norm, state_max, prior_keys, prior_values,
    prior_igate, prior_fgate, accepted,
):
    B, T, D = tokens.shape
    HL, DK = state_matrix.shape[1:3]
    NZ = lax.axis_size("kv") // CORES
    TPN = lax.axis_size("tp")
    BP = -(-B // 8) * 8
    R = T * BP
    W = w_query.shape[1]
    CW = W // 2
    KC = w_query.shape[0]
    ZC = KC * CORES
    OC = w_out.shape[1]
    OW = D // TPN
    VM = pl.BlockSpec(memory_space=pltpu.VMEM)
    HB = pl.BlockSpec(memory_space=pl.ANY)
    V, DMA = pltpu.VMEM, pltpu.SemaphoreType.DMA
    NS = NZ // 2 + 1
    outs = pl.pallas_call(
        functools.partial(kernel, (B, T, BP, NZ, TPN, HL, DK)),
        out_shape=(
            jax.ShapeDtypeStruct((T, B, OW), F32),
            jax.ShapeDtypeStruct(state_matrix.shape, F32),
            jax.ShapeDtypeStruct(state_norm.shape, F32),
            jax.ShapeDtypeStruct((HL, B), F32),
        ),
        in_specs=[HB, VM, HB, HB, HB, HB, HB, VM, VM, VM, HB, HB, HB, VM, HB, HB, VM, VM, VM],
        out_specs=(VM, HB, VM, VM),
        scratch_shapes=[
            V((T, B, D), BF16), V((T, BP, D), F32), V((NZ, 2 * R, ZC), BF16),
            V((D, 3 * CW), BF16), V((NZ, W, CORES * OC), BF16), V((2 * R, 3 * CW), F32),
            V(state_matrix.shape, F32), V(state_matrix.shape, BF16),
            V((T, B, W), BF16), V((T, B, W), BF16), V(state_norm.shape, F32),
            V((HL, D), BF16), V((HL, D), BF16),
            V((HL, BP * 8, DK), F32), V((HL, BP * 8, DK), F32),
            V((HL, BP * 8, DK), F32), V((HL, BP * 8, DK), F32),
            V((HL, 2, R, DK), F32), V((8, R), F32), V((HL, BP, DK), F32), V((HL, BP, DK), F32),
            V((3, 2, R, CW), BF16), V((3, R, CW), BF16), V((R, W), BF16),
            V((TPN - 1, R, OW), BF16), V((TPN - 1, R, OW), BF16), V((R, OW), F32),
            DMA((12,)), DMA((5, 2, NS)), DMA((5, 2, NS)), DMA((5, 2, NS)), DMA((5, 2, NS)),
            DMA((NZ,)), DMA((NZ,)), DMA((3,)), DMA((3,)), DMA((TPN - 1,)), DMA((TPN - 1,)),
            DMA((B,)),
        ],
        compiler_params=pltpu.CompilerParams(
            collective_id=0, has_side_effects=True, vmem_limit_bytes=60 * 1024 * 1024
        ),
        name="cell",
    )(
        tokens.transpose(1, 0, 2), norm_gain.reshape(1, -1), w_query, w_key, w_value,
        w_igate.T, w_fgate.T, igate_bias.reshape(1, -1), fgate_bias.reshape(1, -1),
        head_gain.reshape(1, -1), w_out, state_matrix, state_norm, state_max.T,
        prior_keys.transpose(1, 0, 2), prior_values.transpose(1, 0, 2),
        prior_igate.transpose(1, 2, 0), prior_fgate.transpose(1, 2, 0), accepted.reshape(1, -1),
    )
    mixed, new_matrix, new_norm, new_max = outs
    return mixed.transpose(1, 0, 2), new_matrix, new_norm, new_max.T


def solution(mesh):
    rows = ("grp", "kv")
    return jax.shard_map(
        body,
        mesh=mesh,
        in_specs=(
            P(rows, None, None), P(), P("kv", "tp"), P("kv", "tp"), P("kv", "tp"),
            P(None, "tp"), P(None, "tp"), P("tp"), P("tp"), P("tp"), P("tp", "kv"),
            P(rows, "tp", None, None), P(rows, "tp", None), P(rows, "tp"),
            P(rows, None, "tp"), P(rows, None, "tp"), P(rows, None, "tp"), P(rows, None, "tp"),
            P(rows),
        ),
        out_specs=(
            P(rows, None, "tp"), P(rows, "tp", None, None), P(rows, "tp", None), P(rows, "tp"),
        ),
        check_vma=False,
    )
```

time: 234 us -> 126 us (0.54)
  the two profiles are of different devices: /device:TPU:43 before, /device:TPU:33 now
where the time goes in v1:
time: 126 us
  Pallas kernels  114 us (90%)
  local copies, waits for them, and re-layouts  11.6 us (9%)
    pallas_call x1, Pallas kernels, body(): pl.pallas_call(functools.partial(kernel, (B, T, BP, NZ, TPN, HL, DK)), ou...  114 us
    unnamed x8, local copies, waits for them, and re-layouts  9.03 us

profile of v1, /device:TPU:33, one launch (start us, length us, event | category | flops | bytes accessed | tf_op | source)
XLA Modules:
  0.0 126.1 jit_solution(17191726965523162417)
XLA Ops:
  0.6 1.3 reshape.26.hgain
  1.9 1.3 %reshape.23.ngain = bf16[1,4096]{1,0:T(2,128)(2,1)} reshape(bf16[4096]{0:T(1024)(128)(2,1)} %param.20) | data formatting | bytes 16384 | tf_op jit(solution)/shard_map/reshape | solution.py:463
  3.2 113.9 %cell.1 = (f32[6,22,1024]{2,1,0:T(8,128)}, f32[22,4,128,128]{3,2,1,0:T(8,128)}, f32[22,4,128]{2,1,0:T(4,128)}, f32[4,22]{1,0:T(4,128)}) custom-call(bf16[6,22,4096]{2,1,0:T(8,128)(2,1)} %bitcast.13, bf16[1,4096]{1,0:T(2,128)(2,1)} %reshape.23.ngain, bf16[128,512]{1,0:T(8,128)(2,1)} %wq_h.1, bf16[128,512]{1,0:T(8,128)(2,1)} %wk_h.1, bf16[128,512]{1,0:T(8,128)(2,1)} %wv_h.1, ...), custom_call_target="tpu_custom_call" | custom-call | tf_op jit(solution)/shard_map/cell/pallas_call | solution.py:433
  117.1 1.9 %copy.27 = f32[22,6,1024]{2,0,1:T(8,128)} copy(f32[22,6,1024]{2,0,1:T(8,128)} %bitcast.14) | data formatting | bytes 1081344
  119.0 0.0 copy-start
  119.0 0.0 copy-start.1
  119.0 5.9 %copy.28 = f32[22,4,128,128]{3,2,1,0:T(8,128)} copy(f32[22,4,128,128]{3,2,1,0:T(8,128)} %get-tuple-element.17) | data formatting | bytes 11534336
  124.9 0.0 copy-done
  124.9 0.6 copy.29
  125.5 0.0 copy-done.1
  125.5 0.6 copy.30
Async XLA Ops:
  119.0 5.9 %copy-start = (f32[22,4,128]{2,1,0:T(4,128)S(1)}, f32[22,4,128]{2,1,0:T(4,128)}, u32[]{:S(2)}) copy-start(f32[22,4,128]{2,1,0:T(4,128)} %get-tuple-element.18) | copy-start | bytes 135172
  119.0 6.5 %copy-start.1 = (f32[4,22]{1,0:T(4,128)S(1)}, f32[4,22]{1,0:T(4,128)}, u32[]{:S(2)}) copy-start(f32[4,22]{1,0:T(4,128)} %get-tuple-element.11) | copy-start | bytes 1060

commit v2 on v1

v2 whole, which is shorter than its diff:
```python
import functools

import jax
import jax.numpy as jnp
from jax import lax
from jax.experimental import pallas as pl
from jax.experimental.pallas import tpu as pltpu
from jax.sharding import PartitionSpec as P

EPS = 1e-06
F32, BF16 = jnp.float32, jnp.bfloat16
MESH = pl.DeviceIdType.MESH
CORES = 2
HIGH = lax.Precision.HIGHEST
LAST = (((1,), (1,)), ((), ()))


def log_sigmoid(v):
    return jnp.minimum(v, 0.0) - jnp.log1p(jnp.exp(-jnp.abs(v)))


def kernel(
    dims,
    tok_h, ngain, wq_h, wk_h, wv_h, wig_h, wfg_h, igb, fgb, hgain, wo_h, st_h, sn_h, smax,
    pk_h, pv_h, pig, pfg, acc_n,
    mixed, st, nnorm, nmax,
    tok, xf, xb, wg, wo, acc, sb, pk, pv, sn, wig, wfg, kwb, vb, qb, qsb, gr, gc, ab, nrm,
    g32, h32, qall, sendq, hid, rout, rin, part,
    loc, zs, zr, dsn, drc, drw, xs, xr, ys, yr, fs, fr_sem, qs_sem, qr_sem, rs_sem, rr_sem,
    left_in, twin_in, mate_in, tp_in,
):
    B, T, BP, NZ, TPN, HL, DK = dims
    R = T * BP
    g, kv, tp = lax.axis_index("grp"), lax.axis_index("kv"), lax.axis_index("tp")
    z, c = kv // CORES, lax.rem(kv, CORES)
    par = lax.rem(g, 2)
    mate = g + 1 - 2 * par
    KC = wq_h.shape[0]
    ZC = CORES * KC
    CW = wq_h.shape[1] // 2
    OC = wo_h.shape[1]
    HO = wo_h.shape[0] // 2
    N1 = (NZ - 1) * 3 // 5
    N0 = NZ - 1 - N1
    LATE = 4
    LAG = 2
    SLOTS = max(N1, N0 + LATE)
    corner = (z == 0) & (tp == 0)
    first = corner & (par == 0) & (c == 0)
    hold_twin = corner & (par == 0) & (c == 1)
    hold_mate = corner & (par == 1) & (c == 0)
    hold_sum = hold_twin | hold_mate
    hold_left = ((z == 0) & jnp.logical_not(first)) | (
        (z == 1) & (tp == 0) & (par == 0) & (c == 0)
    )
    prompt = jnp.where((tp == 0) & (par == 0), z - 1, z)

    def up(s):
        return lax.rem(z + s, NZ)

    def down(s):
        return lax.rem(z + NZ - s, NZ)

    def has1(k):
        return (k >= 1) & (k <= N1)

    def hop0(k):
        return jnp.where(k <= prompt, k, k - LATE)

    def has0(k):
        early = (k >= 1) & (k <= prompt) & (k <= N0)
        late = (k > prompt) & (k - LATE > prompt) & (k - LATE >= 1) & (k - LATE <= N0)
        return early | late

    ring_to = (up(1) * CORES + c, down(1) * CORES + c)
    twin = z * CORES + 1 - c

    def remote(src, dst, send, recv, dev):
        return pltpu.make_async_remote_copy(
            src_ref=src, dst_ref=dst, send_sem=send, recv_sem=recv,
            device_id=dev, device_id_type=MESH,
        )

    def slot(item, zz, cc, half):
        return wg.at[zz, item, cc] if item < 3 else wo.at[zz, cc, half]

    def zcopy(item, way, zz):
        ref = slot(item, zz, c, par)
        return remote(ref, ref, zs.at[item, way], zr.at[item, zz], {"kv": ring_to[way]})

    def dcopy(item, zz, cc):
        ref = slot(item, zz, cc, par)
        recv = drc.at[zz] if item < 3 else drw
        return remote(ref, ref, dsn.at[item], recv, {"kv": twin})

    def ycopy(zz, half):
        ref = wo.at[zz, c, half]
        return remote(ref, ref, ys, yr.at[zz], {"grp": mate})

    def fcopy(zz, cc):
        ref = wo.at[zz, cc, 1 - par]
        return remote(ref, ref, fs, fr_sem, {"kv": twin})

    def xcopy(zz, lo, hi):
        return remote(
            xb.at[zz, pl.ds(lo, R), :], xb.at[zz, pl.ds(hi, R), :], xs, xr.at[zz],
            {"grp": mate},
        )

    def onward(item, way, zz):
        zcopy(item, way, zz).start()

    def send_x():
        xcopy(z, 0, R).start()
        for s in range(1, N1 + 1):
            xcopy(up(s), 0, R).start()
            if s <= N0:
                xcopy(down(s), 0, R).start()

    def to_mate(item, zz):
        if item == 3:
            @pl.when(zz != z)
            def _():
                ycopy(zz, par).start()

    def to_twin(item, zz):
        dcopy(item, zz, c).start()
        if item == 3:
            @pl.when(zz == z)
            def _():
                fcopy(zz, c).start()

    def arrive(items, k, defer):
        low = hop0(k)
        zz1, zz0 = up(k), down(low)
        past = k > defer
        for item in items:
            @pl.when(has1(k))
            def _():
                zcopy(item, 1, zz1).wait_recv()

                @pl.when((k < N1) & (jnp.logical_not(hold_left) | past))
                def _():
                    onward(item, 1, zz1)

                @pl.when(jnp.logical_not(hold_twin) | past)
                def _():
                    to_twin(item, zz1)

                @pl.when(jnp.logical_not(hold_mate) | past)
                def _():
                    to_mate(item, zz1)

            @pl.when(has0(k))
            def _():
                zcopy(item, 0, zz0).wait_recv()

                @pl.when(low < N0)
                def _():
                    onward(item, 0, zz0)

                to_twin(item, zz0)
                to_mate(item, zz0)

        for hold, met, send in (
            (hold_left, lambda: pl.semaphore_wait(left_in, 1), lambda i, zz: onward(i, 1, zz)),
            (hold_twin, lambda: pl.semaphore_wait(twin_in, 1), to_twin),
            (hold_mate, lambda: pl.semaphore_wait(mate_in, 1), to_mate),
        ):
            @pl.when(hold & (k == defer))
            def _():
                if 3 not in items:
                    met()
                    if send is to_mate:
                        send_x()
                for s in range(defer + 1):
                    for item in items:
                        send(item, up(s))

    def begin(items):
        for item in items:
            onward(item, 0, z)

            @pl.when(jnp.logical_not(hold_left))
            def _():
                onward(item, 1, z)

            @pl.when(jnp.logical_not(hold_twin))
            def _():
                to_twin(item, z)

    def hand_over(k):
        @pl.when(has1(k))
        def _():
            ycopy(up(k), 1 - par).wait_recv()
            fcopy(up(k), c).start()

        @pl.when(has0(k))
        def _():
            ycopy(down(hop0(k)), 1 - par).wait_recv()
            fcopy(down(hop0(k)), c).start()

    def product(zz):
        both = wg.at[zz, :, 1 - c]
        remote(both, both, dsn.at[0], drc.at[zz], {"kv": twin}).wait_recv()
        xcopy(zz, R, R).wait_recv()
        x = xb[zz]
        return [
            jnp.dot(x, wg[zz, j].reshape(ZC, CW), preferred_element_type=F32) for j in range(3)
        ]

    def add_product(zz):
        for j, v in enumerate(product(zz)):
            acc[j] += v

    def products(k):
        @pl.when(has1(k))
        def _():
            add_product(up(k))

        @pl.when(has0(k))
        def _():
            add_product(down(hop0(k)))

    c0 = pl.multiple_of(par * CW, CW)
    mine = [
        pltpu.make_async_copy(src.at[:, pl.ds(c0, CW)], wg.at[z, i, c], loc.at[i])
        for i, src in enumerate((wq_h, wk_h, wv_h))
    ] + [
        pltpu.make_async_copy(wo_h.at[pl.ds(i * HO, HO), :], wo.at[z, c, i], loc.at[3 + i])
        for i in range(2)
    ]
    loads = [
        pltpu.make_async_copy(src, dst, loc.at[5 + i])
        for i, (src, dst) in enumerate((
            (tok_h, tok), (wig_h, wig), (wfg_h, wfg), (pk_h, pk), (pv_h, pv), (sn_h, sn), (st_h, st),
        ))
    ]
    barrier = pltpu.get_barrier_semaphore()

    def signal(sem, dev):
        pl.semaphore_signal(sem, inc=1, device_id=dev, device_id_type=MESH)

    right, left = lax.rem(tp + 1, TPN), lax.rem(tp + TPN - 1, TPN)
    tops, tops_l = tp < right, tp < left
    signal(barrier, {"kv": ring_to[1]})
    for cond, dev in (
        (c == 1, {"kv": twin}), (par == 1, {"grp": mate}),
        (jnp.logical_not(tops), {"tp": right}), (jnp.logical_not(tops_l), {"tp": left}),
    ):
        @pl.when(cond)
        def _():
            signal(barrier, dev)

    for cp in mine + loads:
        cp.start()
    for cp in mine:
        cp.wait()
    one = lambda cond: jnp.where(cond, 1, 0)
    pl.semaphore_wait(barrier, 1 + one(c == 0) + one(par == 0) + one(tops) + one(tops_l))
    signal(left_in, {"kv": ring_to[0]})
    for cond, sem, dev in (
        (c == 0, twin_in, {"kv": twin}), (par == 0, mate_in, {"grp": mate}),
        (tops, tp_in.at[0], {"tp": right}), (tops_l, tp_in.at[1], {"tp": left}),
    ):
        @pl.when(cond)
        def _():
            signal(sem, dev)

    @pl.when(jnp.logical_not(hold_left))
    def _():
        pl.semaphore_wait(left_in, 1)

    @pl.when((c == 1) & jnp.logical_not(hold_twin))
    def _():
        pl.semaphore_wait(twin_in, 1)

    @pl.when((par == 1) & jnp.logical_not(hold_mate))
    def _():
        pl.semaphore_wait(mate_in, 1)

    begin((0, 1, 2))

    loads[0].wait()
    g32[...] = ngain[...].astype(F32)
    h32[:HL] = hgain[...].astype(F32)
    xf[...] = jnp.zeros_like(xf)

    def norm_rows(t, carry):
        v = tok[t].astype(F32)
        xf[t, :B, :] = v * lax.rsqrt(jnp.mean(v * v, axis=-1, keepdims=True) + EPS)
        return carry

    lax.fori_loop(0, T, norm_rows, 0)
    LN = 128

    def cut_rows(i, carry):
        for j in range(ZC // LN):
            cols = pl.ds(pl.multiple_of(i * ZC + j * LN, LN), LN)
            v = xf[:, :, cols].reshape(R, LN) * g32[pl.ds(i * (ZC // LN) + j, 1), :]
            xb[i, :R, j * LN : (j + 1) * LN] = v.astype(BF16)
        return carry

    lax.fori_loop(0, NZ, cut_rows, 0)

    @pl.when(jnp.logical_not(hold_mate))
    def _():
        send_x()

    loads[1].wait()
    loads[2].wait()

    def gates(i, carry):
        a1, b0, b1 = carry
        cols = pl.ds(pl.multiple_of(i * ZC, ZC), ZC)
        xi, wi, wf = xb[i, :R, :], wig[:, cols], wfg[:, cols]
        dot = functools.partial(lax.dot_general, dimension_numbers=LAST, preferred_element_type=F32)
        return a1 + dot(xi, wf), b0 + dot(wi, xi), b1 + dot(wf, xi)

    zc_ = jnp.zeros((HL, R), F32)
    fr, ic, fc = lax.fori_loop(0, NZ, gates, (jnp.zeros((R, HL), F32), zc_, zc_))
    r0 = lax.broadcasted_iota(jnp.int32, (R, R), 0)
    r1 = lax.broadcasted_iota(jnp.int32, (R, R), 1)
    same = lax.rem(r0, BP) == lax.rem(r1, BP)
    upto = jnp.where(same & (r0 >= r1), 1.0, 0.0).astype(F32)
    cum_r = jnp.dot(
        upto, log_sigmoid(fr + fgb[...]), precision=HIGH, preferred_element_type=F32
    )
    lane_of = lambda ref: jnp.concatenate(
        [jnp.broadcast_to(ref[:, h : h + 1], (1, R)) for h in range(HL)], axis=0
    )
    cum_c = lax.dot_general(
        log_sigmoid(fc + lane_of(fgb)), upto, LAST, precision=HIGH, preferred_element_type=F32
    )
    gc[:HL, :] = ic + lane_of(igb) - cum_c

    lf, ig, run = [], [], None
    for t in range(T):
        live = t < acc_n[...]
        f = jnp.where(live, log_sigmoid(pfg[t]), 0.0)
        run = f if run is None else run + f
        lf.append(run)
        ig.append(jnp.where(live, pig[t], -1e30))
    wlog = [run - lf[t] + ig[t] for t in range(T)]
    top = functools.reduce(jnp.maximum, wlog)
    new_max = jnp.maximum(run + smax[...], top)
    nmax[...] = new_max
    eye = jnp.where(
        lax.broadcasted_iota(jnp.int32, (BP, B), 0) == lax.broadcasted_iota(jnp.int32, (BP, B), 1),
        1.0, 0.0,
    ).astype(F32)
    turn = lambda v: lax.dot_general(eye, v, LAST, precision=HIGH, preferred_element_type=F32)
    carry_r = turn(jnp.exp(run + smax[...] - new_max))
    max_r = turn(new_max)
    wts = [turn(jnp.exp(wlog[t] - new_max)) * (DK**-0.5) for t in range(T)]
    for h in range(HL):
        ab[h] = jnp.broadcast_to(carry_r[:, h : h + 1], (BP, DK))
        gr[h, 0] = jnp.broadcast_to(cum_r[:, h : h + 1], (R, DK))
        for t in range(T):
            gr[h, 1, t * BP : (t + 1) * BP] = jnp.broadcast_to(max_r[:, h : h + 1], (BP, DK))

    for cp in loads[3:6]:
        cp.wait()
    for ref in (kwb, vb, qb):
        ref[...] = jnp.zeros_like(ref)
    for h in range(HL):
        cols = slice(h * DK, (h + 1) * DK)
        total = None
        for t in range(T):
            kw = pk[t, :, cols].astype(F32) * wts[t][:B, h : h + 1]
            kwb[h, pl.ds(t, B, stride=8), :] = kw
            vb[h, pl.ds(t, B, stride=8), :] = pv[t, :, cols].astype(F32)
            total = kw if total is None else total + kw
        nrm[h, :B] = total
    for b in range(B):
        for h in range(HL):
            row = ab[h, b : b + 1] * sn[b, h : h + 1] + nrm[h, b : b + 1]
            nrm[h, b : b + 1] = row
            nnorm[b, h : h + 1] = row
    loads[6].wait()

    def fold(b):
        rows = pl.ds(pl.multiple_of(b * 8, 8), 8)
        for h in range(HL):
            outer = lax.dot_general(
                kwb[h, rows, :].astype(BF16), vb[h, rows, :].astype(BF16),
                (((0,), (0,)), ((), ())), preferred_element_type=F32,
            )
            s = st[b, h] * ab[h, pl.ds(b, 1), :] + outer
            st[b, h] = s
            sb[b, h] = s.astype(BF16)

    per = B // SLOTS
    for b in range(per * SLOTS, B):
        fold(b)

    acc[...] = jnp.zeros_like(acc)

    @pl.when(jnp.logical_not(hold_sum))
    def _():
        add_product(z)

    def ring(k, carry):
        arrive((0, 1, 2), k, LATE)

        @pl.when(k == LAG)
        def _():
            begin((3,))

        arrive((3,), k - LAG, LATE - LAG)

        @pl.when(jnp.logical_not(hold_sum) | (k > LATE + 1))
        def _():
            products(k - 1)

        @pl.when(hold_sum & (k == LATE + 1))
        def _():
            lax.fori_loop(0, LATE + 1, lambda s, c_: (add_product(up(s)), c_)[1], 0)

        for i in range(per):
            fold((k - 1) * per + i)
        return carry

    lax.fori_loop(1, SLOTS + 1, ring, 0)
    products(SLOTS)
    qcopies = []
    for j in range(3):
        sendq[j] = acc[j, R:].astype(BF16)
        cp = remote(
            sendq.at[j], qall.at[j, par], qs_sem.at[j], qr_sem.at[j], {"grp": mate}
        )
        cp.start()
        qcopies.append(cp)
        qall[j, par] = acc[j, :R].astype(BF16)

    def out_slot(k):
        arrive((3,), jnp.int32(k - LAG), LATE - LAG)

    keep = same & (r0 >= r1) & (lax.rem(r1, BP) < B)

    def spread(half, i):
        h = half * 2 + i
        q = qall[0, half, :, i * DK : (i + 1) * DK].astype(F32)
        for t in range(T):
            qb[h, pl.ds(t, BP, stride=8), :] = q[t * BP : (t + 1) * BP]
        for b in range(B):
            rows = slice(b * 8, b * 8 + 8)
            qsb[h, rows, :] = jnp.dot(
                qb[h, rows, :].astype(BF16), sb[b, h], preferred_element_type=F32
            )

    def head(half, i):
        h = half * 2 + i
        cols = slice(i * DK, (i + 1) * DK)
        q, k, v = (qall[j, half, :, cols] for j in range(3))
        cum = gr[h, 0, :, :1]
        inter = cum + gr[h, 1, :, :1]
        decay = jnp.where(keep, cum + gc[pl.ds(h, 1), :], -1e30)
        top_r = jnp.maximum(inter, jnp.max(decay, axis=1, keepdims=True))
        scale = jnp.exp(inter - top_r)
        scores = lax.dot_general(q, k, LAST, preferred_element_type=F32) * (DK**-0.5)
        scores = scores * jnp.exp(decay - top_r)
        q32 = q.astype(F32)
        nh = nrm[h]
        read = jnp.concatenate(
            [qsb[h, pl.ds(t, BP, stride=8), :] for t in range(T)], axis=0
        )
        qn = jnp.concatenate(
            [
                jnp.sum(q32[t * BP : (t + 1) * BP] * nh, axis=1, keepdims=True)
                for t in range(T)
            ],
            axis=0,
        )
        num = scale * read + jnp.dot(scores.astype(BF16), v, preferred_element_type=F32)
        den = scale * qn + jnp.sum(scores, axis=1, keepdims=True)
        cell = num / jnp.maximum(jnp.abs(den), jnp.exp(-top_r))
        cell = cell * lax.rsqrt(jnp.mean(cell * cell, axis=1, keepdims=True) + EPS)
        hc = pl.ds(pl.multiple_of(h * DK, DK), DK)
        hid[:, hc] = (cell * h32[pl.ds(h, 1), :]).astype(BF16)

    nrm[:, B:] = jnp.zeros((HL, BP - B, DK), F32)
    qsb[:, B * 8 :, :] = jnp.zeros((HL, (BP - B) * 8, DK), F32)
    def handed(lo, hi):
        def one_slot(k, carry):
            hand_over(k)
            return carry

        lax.fori_loop(lo, hi, one_slot, 0)

    steps = [
        lambda: (spread(par, 0), spread(par, 1)), lambda: head(par, 0), lambda: head(par, 1),
    ]
    for i in range(LAG):
        with jax.named_scope("outslot"):
            out_slot(SLOTS + 1 + i)
        if i < len(steps):
            steps[i]()
    for f in steps[LAG:]:
        f()
    handed(1, 5)
    for j, cp in enumerate(qcopies):
        cp.wait_send()
        remote(
            sendq.at[j], qall.at[j, 1 - par], qs_sem.at[j], qr_sem.at[j], {"grp": mate}
        ).wait_recv()
    spread(1 - par, 0)
    spread(1 - par, 1)
    head(1 - par, 0)
    head(1 - par, 1)
    with jax.named_scope("handed"):
        handed(5, SLOTS + 1)
    for half, sem in ((par, drw), (1 - par, fr_sem)):
        ref = wo.at[:, 1 - c, half]
        remote(ref, ref, fs, sem, {"kv": twin}).wait_recv()

    @pl.when(jnp.logical_not(tops))
    def _():
        pl.semaphore_wait(tp_in.at[1], 1)

    @pl.when(jnp.logical_not(tops_l))
    def _():
        pl.semaphore_wait(tp_in.at[0], 1)

    per_tp = NZ // TPN
    NB = CORES * OC
    HW = per_tp * NB // 2

    def block(target, i):
        zz = target * per_tp + i
        w = jnp.concatenate(
            [wo[zz, cc].reshape(2 * HO, OC) for cc in range(CORES)], axis=1
        )
        return jnp.dot(hid[...], w, preferred_element_type=F32)

    def chunk(target, half):
        n = per_tp // 2
        return jnp.concatenate([block(target, half * n + i) for i in range(n)], axis=1)

    def rcopy(i):
        return remote(
            rout.at[i], rin.at[i], rs_sem.at[i], rr_sem.at[i],
            {"tp": right if i % 2 == 0 else left},
        )

    far = lax.rem(tp + 2, TPN)
    for i, (target, half) in enumerate(((far, 0), (far, 1), (right, 1), (left, 0))):
        rout[i] = chunk(target, half).astype(BF16)
        rcopy(i).start()
    part[0] = chunk(right, 0)
    part[1] = chunk(left, 1)
    for i in range(2):
        rcopy(i).wait_recv()
        rout[4 + i] = (part[i] + rin[i].astype(F32)).astype(BF16)
        rcopy(4 + i).start()
    for i in range(2):
        part[i] = chunk(tp, i)

    def sent(ref, sem):
        remote(ref, ref, sem, drw, {"kv": twin}).wait_send()

    for item in range(4):
        kind = lambda n: wg.at[pl.ds(0, n), item, 0] if item < 3 else wo.at[pl.ds(0, n), 0, 0]
        sent(kind(N0), zs.at[item, 0])
        sent(kind(N1), zs.at[item, 1])
        sent(kind(NZ), dsn.at[item])
    sent(wo.at[pl.ds(0, NZ - 1), 0, 0], ys)
    sent(wo.at[pl.ds(0, NZ), 0, 0], fs)
    sent(xb.at[:, pl.ds(0, R), :], xs)
    for i in range(6):
        rcopy(i).wait_send()
        if i >= 2:
            rcopy(i).wait_recv()
    for t in range(T):
        rows = slice(t * BP, (t + 1) * BP)
        lo = part[0, rows] + rin[4, rows].astype(F32) + rin[3, rows].astype(F32)
        hi = part[1, rows] + rin[2, rows].astype(F32) + rin[5, rows].astype(F32)
        mixed[t, :, :HW] = lo[:B]
        mixed[t, :, HW:] = hi[:B]


def body(
    tokens, norm_gain, w_query, w_key, w_value, w_igate, w_fgate, igate_bias, fgate_bias,
    head_gain, w_out, state_matrix, state_norm, state_max, prior_keys, prior_values,
    prior_igate, prior_fgate, accepted,
):
    B, T, D = tokens.shape
    HL, DK = state_matrix.shape[1:3]
    NZ = lax.axis_size("kv") // CORES
    TPN = lax.axis_size("tp")
    BP = -(-B // 8) * 8
    R = T * BP
    W = w_query.shape[1]
    CW = W // 2
    KC = w_query.shape[0]
    ZC = KC * CORES
    OC = w_out.shape[1]
    OW = D // TPN
    VM = pl.BlockSpec(memory_space=pltpu.VMEM)
    HB = pl.BlockSpec(memory_space=pl.ANY)
    V, DMA, REG = pltpu.VMEM, pltpu.SemaphoreType.DMA, pltpu.SemaphoreType.REGULAR
    shapes = (
        jax.ShapeDtypeStruct((T, B, OW), F32),
        jax.ShapeDtypeStruct(state_matrix.shape, F32),
        jax.ShapeDtypeStruct(state_norm.shape, F32),
        jax.ShapeDtypeStruct((HL, B), F32),
    )
    outs = pl.pallas_call(
        functools.partial(kernel, (B, T, BP, NZ, TPN, HL, DK)),
        out_shape=tuple(V(a.shape, a.dtype) for a in shapes),
        in_specs=[HB, VM, HB, HB, HB, HB, HB, VM, VM, VM, HB, HB, HB, VM, HB, HB, VM, VM, VM],
        out_specs=(VM, VM, VM, VM),
        scratch_shapes=[
            V((T, B, D), BF16), V((T, BP, D), F32), V((NZ, 2 * R, ZC), BF16),
            V((NZ, 3, CORES, KC, CW), BF16), V((NZ, CORES, 2, W // 2, OC), BF16),
            V((3, 2 * R, CW), F32),
            V(state_matrix.shape, BF16),
            V((T, B, W), BF16), V((T, B, W), BF16), V(state_norm.shape, F32),
            V((HL, D), BF16), V((HL, D), BF16),
            V((HL, BP * 8, DK), F32), V((HL, BP * 8, DK), F32),
            V((HL, BP * 8, DK), F32), V((HL, BP * 8, DK), F32),
            V((HL, 2, R, DK), F32), V((8, R), F32), V((HL, BP, DK), F32), V((HL, BP, DK), F32),
            V((D // 128, 128), F32), V((8, DK), F32),
            V((3, 2, R, CW), BF16), V((3, R, CW), BF16), V((R, W), BF16),
            V((6, R, OW // 2), BF16), V((6, R, OW // 2), BF16), V((2, R, OW // 2), F32),
            DMA((12,)), DMA((4, 2)), DMA((4, NZ)), DMA((4,)), DMA((NZ,)), DMA,
            DMA, DMA((NZ,)), DMA, DMA((NZ,)), DMA, DMA,
            DMA((3,)), DMA((3,)), DMA((6,)), DMA((6,)),
            REG, REG, REG, pltpu.SemaphoreType.REGULAR((2,)),
        ],
        compiler_params=pltpu.CompilerParams(
            collective_id=0, has_side_effects=True, vmem_limit_bytes=56 * 1024 * 1024
        ),
        name="cell",
    )(
        tokens.transpose(1, 0, 2), norm_gain.reshape(-1, 128), w_query, w_key, w_value,
        w_igate.T, w_fgate.T, igate_bias.reshape(1, -1), fgate_bias.reshape(1, -1),
        head_gain.reshape(-1, DK), w_out, state_matrix, state_norm, state_max.T,
        prior_keys.transpose(1, 0, 2), prior_values.transpose(1, 0, 2),
        prior_igate.transpose(1, 2, 0), prior_fgate.transpose(1, 2, 0), accepted.reshape(1, -1),
    )
    mixed, new_matrix, new_norm, new_max = outs
    return mixed.transpose(1, 0, 2), new_matrix, new_norm, new_max.T


def solution(mesh):
    rows = ("grp", "kv")
    return jax.shard_map(
        body,
        mesh=mesh,
        in_specs=(
            P(rows, None, None), P(), P("kv", "tp"), P("kv", "tp"), P("kv", "tp"),
            P(None, "tp"), P(None, "tp"), P("tp"), P("tp"), P("tp"), P("tp", "kv"),
            P(rows, "tp", None, None), P(rows, "tp", None), P(rows, "tp"),
            P(rows, None, "tp"), P(rows, None, "tp"), P(rows, None, "tp"), P(rows, None, "tp"),
            P(rows),
        ),
        out_specs=(
            P(rows, None, "tp"), P(rows, "tp", None, None), P(rows, "tp", None), P(rows, "tp"),
        ),
        check_vma=False,
    )
```

time: 126 us -> 109 us (0.87)
  the two profiles are of different devices: /device:TPU:33 before, /device:TPU:171 now
where the time goes in v2:
time: 109 us
  Pallas kernels  104 us (95%)
  local copies, waits for them, and re-layouts  4.54 us (4%)
    pallas_call x1, Pallas kernels, body(): pl.pallas_call(functools.partial(kernel, (B, T, BP, NZ, TPN, HL, DK)), ou...  104 us
    unnamed x4, local copies, waits for them, and re-layouts  4.54 us

profile of v2, /device:TPU:171, one launch (start us, length us, event | category | flops | bytes accessed | tf_op | source)
XLA Modules:
  0.0 109.2 jit_solution(2548725513379014639)
XLA Ops:
  0.6 104.0 %cell.1 = (f32[6,22,1024]{2,1,0:T(8,128)S(1)}, f32[22,4,128,128]{3,2,1,0:T(8,128)S(1)}, f32[22,4,128]{2,1,0:T(4,128)S(1)}, f32[4,22]{1,0:T(4,128)S(1)}) custom-call(bf16[6,22,4096]{2,1,0:T(8,128)(2,1)} %bitcast.17, bf16[32,128]{1,0:T(8,128)(2,1)} %bitcast.24, bf16[128,512]{1,0:T(8,128)(2,1)} %wq_h.1, bf16[128,512]{1,0:T(8,128)(2,1)} %wk_h.1, ...), custom_call_target="tpu_custom_call" | custom-call | tf_op jit(solution)/shard_map/cell/pallas_call | solution.py:608
  104.6 0.8 copy.27
  105.5 0.6 copy.30
  106.0 0.6 copy.29
  106.7 2.5 %copy.28 = f32[22,4,128,128]{3,2,1,0:T(8,128)} copy(f32[22,4,128,128]{3,2,1,0:T(8,128)S(1)} %get-tuple-element.13) | data formatting | bytes 11534336

commit v3 on v2

--- a/solution.py
+++ b/solution.py
@@ -42,14 +42,14 @@
     HO = wo_h.shape[0] // 2
     N1 = (NZ - 1) * 3 // 5
     N0 = NZ - 1 - N1
-    LATE = 4
+    LATE = 3
     LAG = 2
     SLOTS = max(N1, N0 + LATE)
     corner = (z == 0) & (tp == 0)
     first = corner & (par == 0) & (c == 0)
     hold_twin = corner & (par == 0) & (c == 1)
     hold_mate = corner & (par == 1) & (c == 0)
-    hold_sum = hold_twin | hold_mate
+    hold_sum = first | hold_twin | hold_mate
     hold_left = ((z == 0) & jnp.logical_not(first)) | (
         (z == 1) & (tp == 0) & (par == 0) & (c == 0)
     )
@@ -423,14 +423,20 @@
 
     lax.fori_loop(1, SLOTS + 1, ring, 0)
     products(SLOTS)
-    qcopies = []
+
+    def qcopy(j, i, half):
+        cols = pl.ds(i * DK, DK)
+        return remote(
+            sendq.at[j, :, cols], qall.at[j, half, :, cols], qs_sem.at[j, i], qr_sem.at[j, i],
+            {"grp": mate},
+        )
+
+    for i in range(2):
+        for j in range(3):
+            cols = slice(i * DK, (i + 1) * DK)
+            sendq[j, :, cols] = acc[j, R:, cols].astype(BF16)
+            qcopy(j, i, par).start()
     for j in range(3):
-        sendq[j] = acc[j, R:].astype(BF16)
-        cp = remote(
-            sendq.at[j], qall.at[j, par], qs_sem.at[j], qr_sem.at[j], {"grp": mate}
-        )
-        cp.start()
-        qcopies.append(cp)
         qall[j, par] = acc[j, :R].astype(BF16)
 
     def out_slot(k):
@@ -499,15 +505,13 @@
     for f in steps[LAG:]:
         f()
     handed(1, 5)
-    for j, cp in enumerate(qcopies):
-        cp.wait_send()
-        remote(
-            sendq.at[j], qall.at[j, 1 - par], qs_sem.at[j], qr_sem.at[j], {"grp": mate}
-        ).wait_recv()
-    spread(1 - par, 0)
-    spread(1 - par, 1)
-    head(1 - par, 0)
-    head(1 - par, 1)
+    for i in range(2):
+        with jax.named_scope("qwait"):
+            for j in range(3):
+                qcopy(j, i, par).wait_send()
+                qcopy(j, i, 1 - par).wait_recv()
+        spread(1 - par, i)
+        head(1 - par, i)
     with jax.named_scope("handed"):
         handed(5, SLOTS + 1)
     for half, sem in ((par, drw), (1 - par, fr_sem)):
@@ -625,7 +629,7 @@
             V((6, R, OW // 2), BF16), V((6, R, OW // 2), BF16), V((2, R, OW // 2), F32),
             DMA((12,)), DMA((4, 2)), DMA((4, NZ)), DMA((4,)), DMA((NZ,)), DMA,
             DMA, DMA((NZ,)), DMA, DMA((NZ,)), DMA, DMA,
-            DMA((3,)), DMA((3,)), DMA((6,)), DMA((6,)),
+            DMA((3, 2)), DMA((3, 2)), DMA((6,)), DMA((6,)),
             REG, REG, REG, pltpu.SemaphoreType.REGULAR((2,)),
         ],
         compiler_params=pltpu.CompilerParams(

time: 109 us -> 101 us (0.927)
  the two profiles are of different devices: /device:TPU:171 before, /device:TPU:43 now
where the time goes in v3:
time: 101 us
  Pallas kernels  95.7 us (95%)
  local copies, waits for them, and re-layouts  4.54 us (4%)
    pallas_call x1, Pallas kernels, body(): pl.pallas_call(functools.partial(kernel, (B, T, BP, NZ, TPN, HL, DK)), ou...  95.7 us
    unnamed x4, local copies, waits for them, and re-layouts  4.54 us

profile of v3, /device:TPU:43, one launch (start us, length us, event | category | flops | bytes accessed | tf_op | source)
XLA Modules:
  0.0 100.9 jit_solution(6641343919046151636)
XLA Ops:
  0.6 95.7 %cell.1 = (f32[6,22,1024]{2,1,0:T(8,128)S(1)}, f32[22,4,128,128]{3,2,1,0:T(8,128)S(1)}, f32[22,4,128]{2,1,0:T(4,128)S(1)}, f32[4,22]{1,0:T(4,128)S(1)}) custom-call(bf16[6,22,4096]{2,1,0:T(8,128)(2,1)} %bitcast.17, bf16[32,128]{1,0:T(8,128)(2,1)} %bitcast.24, bf16[128,512]{1,0:T(8,128)(2,1)} %wq_h.1, bf16[128,512]{1,0:T(8,128)(2,1)} %wk_h.1, ...), custom_call_target="tpu_custom_call" | custom-call | tf_op jit(solution)/shard_map/cell/pallas_call | solution.py:612
  96.4 0.8 copy.27
  97.2 0.6 copy.30
  97.8 0.6 copy.29
  98.4 2.5 %copy.28 = f32[22,4,128,128]{3,2,1,0:T(8,128)} copy(f32[22,4,128,128]{3,2,1,0:T(8,128)S(1)} %get-tuple-element.13) | data formatting | bytes 11534336

commit v4 on v3

--- a/solution.py
+++ b/solution.py
@@ -581,6 +581,17 @@
         hi = part[1, rows] + rin[2, rows].astype(F32) + rin[5, rows].astype(F32)
         mixed[t, :, :HW] = lo[:B]
         mixed[t, :, HW:] = hi[:B]
+
+
+def hand_out(mixed_i, nmat_i, nnorm_i, nmax_i, mixed_o, nmat_o, nnorm_o, nmax_o, sems):
+    n = nmat_i.shape[0] // 2
+    pairs = [(nmat_i.at[pl.ds(i * n, n)], nmat_o.at[pl.ds(i * n, n)]) for i in range(2)]
+    pairs += [(mixed_i, mixed_o), (nnorm_i, nnorm_o), (nmax_i, nmax_o)]
+    copies = [pltpu.make_async_copy(a, b, sems.at[i]) for i, (a, b) in enumerate(pairs)]
+    for cp in copies:
+        cp.start()
+    for cp in copies:
+        cp.wait()
 
 
 def body(
@@ -643,7 +654,11 @@
         prior_keys.transpose(1, 0, 2), prior_values.transpose(1, 0, 2),
         prior_igate.transpose(1, 2, 0), prior_fgate.transpose(1, 2, 0), accepted.reshape(1, -1),
     )
-    mixed, new_matrix, new_norm, new_max = outs
+    mixed, new_matrix, new_norm, new_max = pl.pallas_call(
+        hand_out, out_shape=shapes, in_specs=[VM] * 4, out_specs=(HB,) * 4,
+        scratch_shapes=[DMA((5,))], name="hand_out",
+        compiler_params=pltpu.CompilerParams(vmem_limit_bytes=56 * 1024 * 1024),
+    )(*(pltpu.with_memory_space_constraint(a, pltpu.VMEM) for a in outs))
     return mixed.transpose(1, 0, 2), new_matrix, new_norm, new_max.T
 
 

time: 101 us -> 99.3 us (0.983)
  local copies, waits for them, and re-layouts: 4.54 us -> 0 us
  Pallas kernels: 95.7 us -> 98.5 us
    unnamed x4 -> x0, local copies, waits for them, and re-layouts: 4.54 us -> none
    pallas_call x0 -> x1, Pallas kernels: none -> 2.76 us  [body(): pl.pallas_call(hand_out, out_shape=shapes, in_specs=[VM] * 4, out_specs=(...]
where the time goes in v4:
time: 99.3 us; the launch traced here: 99.1 us
  Pallas kernels  98.5 us (99%)
    pallas_call x1, Pallas kernels, body(): pl.pallas_call(functools.partial(kernel, (B, T, BP, NZ, TPN, HL, DK)), ou...  95.7 us
    pallas_call x1, Pallas kernels, body(): pl.pallas_call(hand_out, out_shape=shapes, in_specs=[VM] * 4, out_specs=(...  2.76 us

profile of v4, /device:TPU:43, one launch (start us, length us, event | category | flops | bytes accessed | tf_op | source)
XLA Modules:
  0.0 99.1 jit_solution(2425573347210546948)
XLA Ops:
  0.6 95.7 %cell.1 = (f32[6,22,1024]{2,1,0:T(8,128)S(1)}, f32[22,4,128,128]{3,2,1,0:T(8,128)S(1)}, f32[22,4,128]{2,1,0:T(4,128)S(1)}, f32[4,22]{1,0:T(4,128)S(1)}) custom-call(bf16[6,22,4096]{2,1,0:T(8,128)(2,1)} %bitcast.15, bf16[32,128]{1,0:T(8,128)(2,1)} %bitcast.22, bf16[128,512]{1,0:T(8,128)(2,1)} %wq_h.1, bf16[128,512]{1,0:T(8,128)(2,1)} %wk_h.1, ...), custom_call_target="tpu_custom_call" | custom-call | tf_op jit(solution)/shard_map/cell/pallas_call | solution.py:623
  96.4 2.8 %hand_out.1 = (f32[6,22,1024]{2,1,0:T(8,128)}, f32[22,4,128,128]{3,2,1,0:T(8,128)}, f32[22,4,128]{2,1,0:T(4,128)}, f32[4,22]{1,0:T(4,128)}) custom-call(f32[6,22,1024]{2,1,0:T(8,128)S(1)} %get-tuple-element.12.mixed_i, f32[22,4,128,128]{3,2,1,0:T(8,128)S(1)} %get-tuple-element.13.nmat_i, f32[22,4,128]{2,1,0:T(4,128)S(1)} %get-tuple-element.14.nnorm_i, ...), custom_call_target="tpu_custom_call" | custom-call | tf_op jit(solution)/shard_map/hand_out/pallas_call | solution.py:657
